TPU v7x, 128 devices: a whole 4x4x4 slice. The times are simulated.
128 devices in a mesh: fs: 16 (over z, y), tp: 8 (over x, core).
Axes of the slice: x: 4, y: 4, z: 4, core: 2. Of those that a mesh axis runs over, the one named last changes fastest.
Arguments:
- tokens: bfloat16 [12288, 2048], P('fs'), may hold values from -6 to 6
- routes: int32 [12288, 2], P('fs'), may hold values from 0 to 15, all different within a row; in each aligned block of 768 rows (0 to 767, 768 to 1535, ...) at most 216 rows name the same one
- route_weight: float32 [12288, 2], P('fs'), may hold values from 0.2 to 1
- norm_gain: float32 [2048], P('fs'), may hold values from 0.1 to 1.9
- gate_master: float32 [16, 2048, 4096], P(None, 'fs', 'tp'), may hold values from -0.125 to 0.125
- up_master: float32 [16, 2048, 4096], P(None, 'fs', 'tp'), may hold values from -0.125 to 0.125
- down_master: float32 [16, 4096, 2048], P(None, 'fs', 'tp'), may hold values from -0.09375 to 0.09375
Outputs:
- gate_serve: bfloat16 [16, 2048, 4096], P('fs', None, 'tp')
- up_serve: bfloat16 [16, 2048, 4096], P('fs', None, 'tp')
- down_serve: bfloat16 [16, 4096, 2048], P('fs', 'tp')
- layer_out: bfloat16 [12288, 2048], P('fs', 'tp')
Inputs may be any that keep to these rules, and one draw needn't show every extreme that they name: `routes`: each row names two different experts; among the 768 rows of one index of fs no expert is named by more than 216 rows, a bound that some block reaches.
All inputs are finite; a program needn't handle non-finite values.
Results may differ from a plain program's by a relative error of at most 0.015.
Values may be sent and summed in bfloat16 or wider, within the bound.
A program may use at most 192 MiB of HBM per device.

v0:
```python
import jax
import jax.numpy as jnp
from jax import lax
from jax.sharding import PartitionSpec as P

CAP = 216


def relay_down(down_cast):
    return lax.all_to_all(
        lax.all_to_all(down_cast, "fs", split_axis=0, concat_axis=1, tiled=True),
        "tp",
        split_axis=1,
        concat_axis=2,
        tiled=True,
    )


def body(tokens, routes, route_weight, norm_gain, gate_master, up_master, down_master):
    rows_local = tokens.shape[0]
    model_width = tokens.shape[1]
    experts = gate_master.shape[0]
    values = tokens.astype(jnp.float32)
    normed = (values * lax.rsqrt(jnp.mean(values * values, axis=-1, keepdims=True) + 1e-06)).astype(
        jnp.bfloat16
    )
    row_gain = norm_gain[None, :, None]
    gate_cast = (row_gain * gate_master).astype(jnp.bfloat16)
    up_cast = (row_gain * up_master).astype(jnp.bfloat16)
    down_cast = down_master.astype(jnp.bfloat16)
    gate_serve, up_serve = (
        lax.all_to_all(gate_cast, "fs", split_axis=0, concat_axis=1, tiled=True),
        lax.all_to_all(up_cast, "fs", split_axis=0, concat_axis=1, tiled=True),
    )
    down_serve = relay_down(down_cast)
    chosen = routes.reshape(-1)
    one_hot = (chosen[:, None] == jnp.arange(experts, dtype=jnp.int32)[None, :]).astype(jnp.int32)
    earlier = jnp.cumsum(one_hot, axis=0) - one_hot
    position = jnp.sum(earlier * one_hot, axis=1)
    slot_index = chosen * CAP + position
    doubled = jnp.repeat(normed, 2, axis=0)
    outgoing = jnp.zeros((experts * CAP, model_width), jnp.bfloat16).at[slot_index].set(doubled)
    outgoing = outgoing.reshape(experts, CAP, model_width)
    gate_matrix = gate_serve[0]
    up_matrix = up_serve[0]
    column_count = model_width // lax.axis_size("tp")
    column_share = lax.dynamic_slice_in_dim(
        outgoing, lax.axis_index("tp") * column_count, column_count, 2
    )
    arrived = lax.all_to_all(column_share, "fs", split_axis=0, concat_axis=0, tiled=True)
    stacked = arrived.reshape(-1, column_count)
    incoming = lax.all_gather(stacked, "tp", axis=1, tiled=True)
    gate_pre = jnp.dot(incoming, gate_matrix, preferred_element_type=jnp.float32)
    up_pre = jnp.dot(incoming, up_matrix, preferred_element_type=jnp.float32)
    hidden = (jax.nn.silu(gate_pre) * up_pre).astype(jnp.bfloat16)
    partial_value = jnp.dot(hidden, down_serve[0], preferred_element_type=jnp.float32)
    rounded = lax.optimization_barrier(partial_value.astype(jnp.bfloat16)).astype(jnp.float32)
    rounded = rounded.reshape(-1, CAP, model_width)
    summed = lax.psum_scatter(rounded.astype(jnp.bfloat16), "tp", scatter_dimension=2, tiled=True)
    returned = lax.all_to_all(summed, "fs", split_axis=0, concat_axis=0, tiled=True)
    returned_rows = returned.reshape(experts * CAP, -1)
    picked = returned_rows[slot_index].astype(jnp.float32).reshape(rows_local, 2, -1)
    combined = jnp.sum(picked * route_weight[:, :, None], axis=1).astype(jnp.bfloat16)
    return (gate_serve, up_serve, down_serve, combined)


def solution(mesh):
    placed = (
        P("fs", None),
        P("fs", None),
        P("fs", None),
        P("fs"),
        P(None, "fs", "tp"),
        P(None, "fs", "tp"),
        P(None, "fs", "tp"),
    )
    return jax.shard_map(
        body,
        mesh=mesh,
        in_specs=placed,
        out_specs=(P("fs", None, "tp"), P("fs", None, "tp"), P("fs", "tp", None), P("fs", "tp")),
        check_vma=False,
    )
```

profile of v0, /device:TPU:32, one launch (start us, length us, event | category | flops | bytes accessed | tf_op | source)
XLA Modules:
  0.0 403.3 jit_solution(312590439847986955)
XLA Ops:
  7.2 0.0 all-gather.2.cloned.1.call-start
  7.2 1.0 copy.33
  8.2 0.2 eq.29
  8.5 0.2 eq.25
  8.7 1.3 broadcast_multiply_fusion
  10.0 4.5 %reduce-window.6 = s32[16,12,128]{2,1,0:T(8,128)S(1)} reduce-window(s32[16,12,128]{2,1,0:T(8,128)S(1)} %fusion.4, s32[]{:T(128)} %constant.6.clone.1), window={size=1x1x128 pad=0_0x0_0x127_0}, to_apply=%region_0.0 | reduce-window | flops 3121152 | bytes 196612 | tf_op jit(solution)/shard_map/reduce-window
  14.6 0.4 slice_reduce_fusion
  15.0 0.2 reduce-window.9
  15.2 0.8 broadcast_add_fusion
  15.9 0.9 copy.32
  16.8 0.3 mul.67
  17.1 2.6 fusion.2
  19.6 0.6 fusion.3
  20.2 5.2 %broadcast_in_dim.5 = bf16[768,2,2048]{2,1,0:T(2,128)(2,1)} broadcast(bf16[768,2048]{1,0:T(8,128)(2,1)S(1)} %fusion.3), dimensions={0,2} | broadcast | bytes 9437184 | tf_op jit(solution)/shard_map/broadcast_in_dim | solution.py:41
  25.4 10.2 %reshape.112 = bf16[1536,2048]{1,0:T(8,128)(2,1)} reshape(bf16[768,2,2048]{2,1,0:T(2,128)(2,1)} %broadcast_in_dim.5) | data formatting | bytes 12582912 | tf_op jit(solution)/shard_map/reshape | solution.py:41
  35.7 18.2 %scatter_custom_fusion = bf16[3456,2048]{1,0:T(8,128)(2,1)} fusion(s32[1536]{0:T(1024)S(1)} %fusion.8, bf16[1536,2048]{1,0:T(8,128)(2,1)} %reshape.112, bf16[]{:T(256)} %constant.11.clone.1), kind=kCustom, calls=%fused_computation.6 | custom fusion | bytes 14156288 | tf_op jit(solution)/shard_map/scatter | solution.py:42
  53.9 1.6 constant_dynamic-slice_fusion
  55.5 30.9 %all_to_all.64 = bf16[16,216,256]{2,1,0:T(8,128)(2,1)} all-to-all(bf16[16,216,256]{2,1,0:T(8,128)(2,1)S(1)} %constant_dynamic-slice_fusion), channel_id=1, replica_groups=mesh['fs'=16,'tp'=8] {'fs'}, dimensions={0} | all-to-all | bytes 3538944 | tf_op jit(solution)/shard_map/all_to_all | solution.py:50
  86.4 0.0 all-gather.2.cloned.1.call-update
  86.5 3.8 convert_element_type.45
  90.2 5.5 %all-to-all-start.2 = ((bf16[16,256,256]{2,1,0:T(8,128)(2,1)}), bf16[16,256,256]{2,1,0:T(8,128)(2,1)S(1)}, u32[]{:S(2)}, u32[]{:S(2)}) async-start(bf16[16,256,256]{2,1,0:T(8,128)(2,1)} %convert_element_type.45), calls=%async_computation.2 | async-start | bytes 4194304 | tf_op jit(solution)/shard_map/all_to_all | solution.py:11
  95.8 8.0 %multiply_convert_fusion.1 = (bf16[16,128,512]{2,1,0:T(8,128)(2,1)}, bf16[16,128,512]{2,1,0:T(8,128)(2,1)}) fusion(f32[16,128,512]{2,1,0:T(8,128)} %param.12, f32[128]{0:T(128)S(1)} %copy-done.4, f32[16,128,512]{2,1,0:T(8,128)} %param.11), kind=kLoop, calls=%fused_computation.10 | loop fusion | flops 4194304 | bytes 12583424 | tf_op jit(solution)/shard_map/convert_element_type | solution.py:29
  103.8 20.1 %all-to-all-done.2 = bf16[16,256,256]{2,1,0:T(8,128)(2,1)S(1)} async-done(((bf16[16,256,256]{2,1,0:T(8,128)(2,1)}), bf16[16,256,256]{2,1,0:T(8,128)(2,1)S(1)}, u32[]{:S(2)}, u32[]{:S(2)}) %all-to-all-start.2) | async-done | bytes 2097184 | tf_op jit(solution)/shard_map/all_to_all | solution.py:11
  123.9 6.1 %all-to-all-start = ((bf16[16,128,512]{2,1,0:T(8,128)(2,1)}), bf16[16,128,512]{2,1,0:T(8,128)(2,1)}, u32[]{:S(2)}, u32[]{:S(2)}) async-start(bf16[16,128,512]{2,1,0:T(8,128)(2,1)} %get-tuple-element.17), calls=%async_computation | async-start | bytes 4194304 | tf_op jit(solution)/shard_map/all_to_all | solution.py:32
  130.0 25.1 %copy.42 = bf16[1,4096,256]{2,0,1:T(2,128)(2,1)} copy(bf16[1,4096,256]{2,1,0:T(8,128)(2,1)S(1)} %bitcast.46) | data formatting | bytes 4194304 | tf_op jit(solution)/shard_map/all_to_all | solution.py:11
  155.1 0.5 broadcast.72
  155.6 21.6 %reduce.4 = bf16[4096,256]{1,0:T(8,128)(2,1)S(1)} reduce(bf16[4096,1,256]{2,1,0:T(2,128)(2,1)} %bitcast.43, bf16[]{:T(256)} %broadcast.72), dimensions={1}, to_apply=%bitcast.39.reduce_sub_computation | reduce | bytes 4194306
  177.2 3.2 reshape.120
  180.4 31.5 %all_to_all.65 = bf16[8,2,65536]{2,1,0:T(2,128)(2,1)S(1)} all-to-all(bf16[8,2,65536]{2,1,0:T(2,128)(2,1)} %reshape.120), channel_id=1, replica_groups=mesh['fs'=16,'tp'=8] {'tp'}, dimensions={0} | all-to-all | bytes 4194304 | tf_op jit(solution)/shard_map/all_to_all | solution.py:10
  211.9 7.3 %all-to-all-start.1 = ((bf16[16,128,512]{2,1,0:T(8,128)(2,1)}), bf16[16,128,512]{2,1,0:T(8,128)(2,1)}, u32[]{:S(2)}, u32[]{:S(2)}) async-start(bf16[16,128,512]{2,1,0:T(8,128)(2,1)} %get-tuple-element.16), calls=%async_computation.1 | async-start | bytes 4194304 | tf_op jit(solution)/shard_map/all_to_all | solution.py:33
  219.2 0.3 reduce-scatter.2.cloned.1.call-start
  219.5 4.4 %reshape.121 = bf16[4096,1,256]{2,1,0:T(2,128)(2,1)} reshape(bf16[8,2,65536]{2,1,0:T(2,128)(2,1)S(1)} %all_to_all.65) | data formatting | bytes 4194304
  223.9 2.5 copy.38
  226.4 2.4 copy.31
  228.8 13.2 %fusion.10 = f32[3456,512]{1,0:T(8,128)} fusion(bf16[3456,2048]{1,0:T(8,128)(2,1)} %all-gather.2.cloned.1.call-done, bf16[2048,512]{1,0:T(8,128)(2,1)} %bitcast.8), kind=kOutput, calls=%fused_computation.30 | convolution fusion | flops 7247757312 | bytes 23330816 | tf_op jit(solution)/shard_map/dot_general | solution.py:53
  242.0 6.3 %all-to-all-done.1 = bf16[16,128,512]{2,1,0:T(8,128)(2,1)} async-done(((bf16[16,128,512]{2,1,0:T(8,128)(2,1)}), bf16[16,128,512]{2,1,0:T(8,128)(2,1)}, u32[]{:S(2)}, u32[]{:S(2)}) %all-to-all-start.1) | async-done | bytes 2097184 | tf_op jit(solution)/shard_map/all_to_all | solution.py:33
  248.3 21.7 %convolution_convert_fusion = bf16[3456,2048]{1,0:T(8,128)(2,1)} fusion(bf16[512,2048]{0,1:T(8,128)(2,1)S(1)} %bitcast.49, f32[3456,512]{1,0:T(8,128)} %fusion.10, bf16[3456,2048]{1,0:T(8,128)(2,1)} %all-gather.2.cloned.1.call-done, bf16[2048,512]{1,0:T(8,128)(2,1)} %bitcast.9), kind=kOutput, calls=%fused_computation.2 | convolution fusion | flops 14513209344 | bytes 39583744 | tf_op jit(solution)/shard_map/dot_general | solution.py:56
  270.0 0.0 reduce-scatter.2.cloned.1.call-update
  270.0 78.2 %reduce-scatter.2.cloned.1.call-done = bf16[16,216,256]{2,1,0:T(8,128)(2,1)} async-done(((bf16[16,216,2048]{2,1,0:T(8,128)(2,1)}), bf16[16,216,256]{2,1,0:T(8,128)(2,1)}) %reduce-scatter.2.cloned.1.call-update) | async-done | bytes 1769488 | tf_op jit(solution)/shard_map/reduce_scatter | solution.py:59
  348.2 7.3 %all-to-all-start.5 = ((bf16[16,216,256]{2,1,0:T(8,128)(2,1)}), bf16[16,216,256]{2,1,0:T(8,128)(2,1)S(1)}, u32[]{:S(2)}, u32[]{:S(2)}) async-start(bf16[16,216,256]{2,1,0:T(8,128)(2,1)} %reduce-scatter.2.cloned.1.call-done), calls=%async_computation.6 | async-start | bytes 3538944 | tf_op jit(solution)/shard_map/all_to_all | solution.py:60
  355.6 0.2 copy.36
  355.8 3.9 copy.37
  359.7 20.1 %all-to-all-done.5 = bf16[16,216,256]{2,1,0:T(8,128)(2,1)S(1)} async-done(((bf16[16,216,256]{2,1,0:T(8,128)(2,1)}), bf16[16,216,256]{2,1,0:T(8,128)(2,1)S(1)}, u32[]{:S(2)}, u32[]{:S(2)}) %all-to-all-start.5) | async-done | bytes 1769504 | tf_op jit(solution)/shard_map/all_to_all | solution.py:60
  379.9 4.8 %gather_fusion = bf16[1536,256]{1,0:T(8,128)(2,1)S(1)} fusion(bf16[3456,256]{1,0:T(8,128)(2,1)S(1)} %bitcast.41, s32[2048]{0:T(1024)S(1)} %pad_clamp_fusion), kind=kCustom, calls=%fused_computation | custom fusion | bytes 1579008 | tf_op jit(solution)/shard_map/gather | solution.py:62
  384.6 0.8 reshape.99
  385.4 5.0 %multiply_reduce_fusion = bf16[768,256]{1,0:T(8,128)(2,1)} fusion(f32[768,2,256]{2,1,0:T(2,128)S(1)} %reshape.99, f32[768,2]{1,0:T(8,128)S(1)} %copy.36), kind=kLoop, calls=%fused_computation.12 | loop fusion | flops 589824 | bytes 1972224 | tf_op jit(solution)/shard_map/reduce_sum | solution.py:63
  390.4 3.0 copy.45
  393.4 3.0 copy.46
  (17 shorter events, 0.1 us)
Async XLA Ops:
  7.2 12.5 %copy-start = (bf16[768,2048]{1,0:T(8,128)(2,1)S(1)}, bf16[768,2048]{1,0:T(8,128)(2,1)}, u32[]{:S(2)}) copy-start(bf16[768,2048]{1,0:T(8,128)(2,1)} %param.7) | copy-start | bytes 9437188
  7.2 221.6 %all-gather.2.cloned.1.call-start = ((), (), s32[]{:S(2)}) async-start(), calls=%async_computation.7 | async-start | bytes 15925248 | tf_op jit(solution)/shard_map/all_gather | solution.py:52
  25.4 10.2 %copy-start.2 = (s32[16,12,128]{2,1,0:T(8,128)S(1)}, s32[16,12,128]{2,1,0:T(8,128)}, u32[]{:S(2)}) copy-start(s32[16,12,128]{2,1,0:T(8,128)} %broadcast_add_fusion) | copy-start | bytes 294916
  86.4 9.3 %copy-start.4 = (f32[128]{0:T(128)S(1)}, f32[128]{0:T(128)}, u32[]{:S(2)}) copy-start(f32[128]{0:T(128)} %param.10) | copy-start | bytes 1540
  90.2 33.7 %all-to-all-start.2 = ((bf16[16,256,256]{2,1,0:T(8,128)(2,1)}), bf16[16,256,256]{2,1,0:T(8,128)(2,1)S(1)}, u32[]{:S(2)}, u32[]{:S(2)}) async-start(bf16[16,256,256]{2,1,0:T(8,128)(2,1)} %convert_element_type.45), calls=%async_computation.2 | async-start | bytes 4194304 | tf_op jit(solution)/shard_map/all_to_all | solution.py:11
  123.9 56.5 %all-to-all-start = ((bf16[16,128,512]{2,1,0:T(8,128)(2,1)}), bf16[16,128,512]{2,1,0:T(8,128)(2,1)}, u32[]{:S(2)}, u32[]{:S(2)}) async-start(bf16[16,128,512]{2,1,0:T(8,128)(2,1)} %get-tuple-element.17), calls=%async_computation | async-start | bytes 4194304 | tf_op jit(solution)/shard_map/all_to_all | solution.py:32
  211.9 36.4 %all-to-all-start.1 = ((bf16[16,128,512]{2,1,0:T(8,128)(2,1)}), bf16[16,128,512]{2,1,0:T(8,128)(2,1)}, u32[]{:S(2)}, u32[]{:S(2)}) async-start(bf16[16,128,512]{2,1,0:T(8,128)(2,1)} %get-tuple-element.16), calls=%async_computation.1 | async-start | bytes 4194304 | tf_op jit(solution)/shard_map/all_to_all | solution.py:33
  219.2 129.1 %reduce-scatter.2.cloned.1.call-start = ((), (), s32[]{:S(2)}) async-start(), calls=%async_computation.8 | async-start | bytes 15925248 | tf_op jit(solution)/shard_map/reduce_scatter | solution.py:59
  228.8 19.5 %copy-start.1 = (bf16[1,512,8,256]{1,3,2,0:T(8,128)(2,1)S(1)}, bf16[1,512,8,256]{1,3,2,0:T(8,128)(2,1)}, u32[]{:S(2)}) copy-start(bf16[1,512,8,256]{1,3,2,0:T(8,128)(2,1)} %copy.31) | copy-start | bytes 6291460
  270.0 85.6 %copy-start.3 = (f32[768,2]{0,1:T(2,128)S(1)}, f32[768,2]{0,1:T(2,128)}, u32[]{:S(2)}) copy-start(f32[768,2]{0,1:T(2,128)} %param.9) | copy-start | bytes 18436
  348.2 31.6 %all-to-all-start.5 = ((bf16[16,216,256]{2,1,0:T(8,128)(2,1)}), bf16[16,216,256]{2,1,0:T(8,128)(2,1)S(1)}, u32[]{:S(2)}, u32[]{:S(2)}) async-start(bf16[16,216,256]{2,1,0:T(8,128)(2,1)} %reduce-scatter.2.cloned.1.call-done), calls=%async_computation.6 | async-start | bytes 3538944 | tf_op jit(solution)/shard_map/all_to_all | solution.py:60
Sparse Core Ops, SparseCore 0:
  86.6 77.4 all-gather.1
  270.2 78.0 reduce-scatter.1
where the time goes:
time: 409 us; the launch traced here: 403 us
  waiting for transfers between devices  125 us (31%)
  local copies, waits for them, and re-layouts  92 us (22%)
  blocking collectives  62.5 us (15%)
  other arithmetic  48.4 us (12%)
  matrix products  34.9 us (9%)
  starting transfers between devices  26.6 us (7%)
  between operations  14.2 us (3%)
    reduce_scatter x1, waiting for transfers between devices, body(): lax.psum_scatter(rounded.astype(jnp.bfloat16), 'tp', scatter_dimension=2,...  78.2 us
    all_to_all x1, blocking collectives, relay_down(): lax.all_to_all(lax.all_to_all(down_cast, 'fs', split_axis=0, concat_axis=...  31.5 us
    all_to_all x1, blocking collectives, body(): lax.all_to_all(column_share, 'fs', split_axis=0, concat_axis=0, tiled=True)  30.9 us
    all_to_all x1, local copies, waits for them, and re-layouts, relay_down(): lax.all_to_all(down_cast, 'fs', split_axis=0, concat_axis=1, tiled=True)  25.1 us
    unnamed x19, local copies, waits for them, and re-layouts  21.9 us
    dot_general x1, matrix products, body(): jnp.dot(hidden, down_serve[0], preferred_element_type=jnp.float32)  21.7 us
    unnamed x1, other arithmetic  21.6 us
    all_to_all x1, waiting for transfers between devices, body(): lax.all_to_all(summed, 'fs', split_axis=0, concat_axis=0, tiled=True)  20.1 us
  transfers between devices with their start and end apart: 6, of which 4 were waited for; matrix products, arithmetic and copies ran while one was open for 22% of the time, Pallas kernels for 0%

commit v1 on v0

v1 whole, which is shorter than its diff:
```python
import functools

import jax
import jax.numpy as jnp
from jax import lax
from jax.experimental import pallas as pl
from jax.experimental.pallas import tpu as pltpu
from jax.sharding import PartitionSpec as P

CAP = 216
MESH = pl.DeviceIdType.MESH
BF = jnp.bfloat16
F32 = jnp.float32
EARLY = 7


def kernel(
    tok_h, rt_ref, wt_ref, gain_ref, gate_h, up_h, down_h,
    gate_o, up_o, down_o, out_ref,
    X, RB, D2, FA, FB, RET, PS, H,
    gate_s, up_s, down_s, gate_r, up_r, down_r,
    st_a, st_d, tok, nrm, acc, pos_e, cols,
    ld, gs, gr, us, ur, ds, dr, ps, xr, ag,
    dds, ddr, s2s, s2r, sas, sar, sbs, sbr, rts, rtr, osem,
):
    fs, tp = lax.axis_index("fs"), lax.axis_index("tp")
    z, y = fs // 4, fs % 4
    x, c = tp // 2, tp % 2
    oc = 1 - c

    def to(s):
        dy = s % 4
        dz = (s // 4 + dy) % 4
        return ((z + dz) % 4) * 4 + (y + dy) % 4

    def of(s):
        dy = s % 4
        dz = (s // 4 + dy) % 4
        return ((z + 4 - dz) % 4) * 4 + (y + 4 - dy) % 4

    def at_x(d):
        return (x + d) % 4

    def lane(d, core):
        return at_x(d) * 2 + core

    sib = (fs, x * 2 + oc)

    def rc(src, dst, ss, rs, dev):
        return pltpu.make_async_remote_copy(
            src_ref=src, dst_ref=dst, send_sem=ss, recv_sem=rs, device_id=dev, device_id_type=MESH
        )

    l_gate = pltpu.make_async_copy(gate_h, st_a, ld.at[0])
    l_tok = pltpu.make_async_copy(tok_h, tok, ld.at[1])
    l_down = pltpu.make_async_copy(down_h, st_d, ld.at[2])
    l_up = pltpu.make_async_copy(up_h, st_a, ld.at[3])
    l_gate.start()
    l_tok.start()
    l_down.start()

    bar = pltpu.get_barrier_semaphore()

    def sig(dev):
        pl.semaphore_signal(bar, inc=1, device_id=dev, device_id_type=MESH)

    self_down = fs // 2 == tp

    @pl.loop(1, 16)
    def _(s):
        sig((to(s), tp))
        sig((to(s), fs // 2))

    sig(sib)
    sig((fs, lane(1, c)))
    sig((fs, lane(3, c)))

    @pl.when(jnp.logical_not(self_down))
    def _():
        sig((fs, fs // 2))

    @pl.loop(0, 16)
    def _(k):
        i, j = tp * 2 + k // 8, k % 8

        @pl.when(jnp.logical_or(i != fs, j != tp))
        def _():
            sig((i, j))

    e_id = lax.broadcasted_iota(jnp.int32, (16, 768), 0)
    m0 = e_id == rt_ref[0:1, :]
    m1 = e_id == rt_ref[1:2, :]
    mt = jnp.logical_or(m0, m1)
    before = (
        lax.broadcasted_iota(jnp.int32, (768, 768), 0) < lax.broadcasted_iota(jnp.int32, (768, 768), 1)
    )
    count = jnp.dot(
        jnp.where(mt, 1.0, 0.0).astype(BF), jnp.where(before, 1.0, 0.0).astype(BF), preferred_element_type=F32
    )
    pos_e[...] = jnp.where(mt, count, -1.0)
    slot = count + (e_id * CAP).astype(F32)
    slot0 = jnp.sum(jnp.where(m0, slot, 0.0), axis=0, keepdims=True)
    slot1 = jnp.sum(jnp.where(m1, slot, 0.0), axis=0, keepdims=True)
    row = lax.broadcasted_iota(jnp.int32, (128, 768), 0)
    table = jnp.where(
        row == 0, slot0, jnp.where(row == 1, slot1, jnp.where(row == 2, wt_ref[0:1, :], wt_ref[1:2, :]))
    )
    cols[...] = table.T

    r128 = lax.broadcasted_iota(jnp.int32, (128, 128), 0)
    c128 = lax.broadcasted_iota(jnp.int32, (128, 128), 1)
    gain = jnp.sum(jnp.where(r128 == c128, gain_ref[...], 0.0), axis=1, keepdims=True)
    mine = pl.ds(pl.multiple_of(fs * 128, 128), 128)

    l_gate.wait()

    @pl.loop(0, 16)
    def _(e):
        gate_s[e] = (st_a[e] * gain).astype(BF)

    gate_r[mine, :] = gate_s[fs]
    l_up.start()

    @pl.when(self_down)
    def _():
        pl.semaphore_wait(bar, 48)

    @pl.when(jnp.logical_not(self_down))
    def _():
        pl.semaphore_wait(bar, 50)

    def gate_copy(s):
        return rc(gate_s.at[to(s)], gate_r.at[mine], gs.at[s], gr.at[fs], (to(s), tp))

    def up_copy(s):
        return rc(up_s.at[to(s)], up_r.at[mine], us.at[s], ur.at[fs], (to(s), tp))

    def down_copy(s):
        return rc(
            down_s.at[to(s)], down_r.at[fs % 2, tp], ds.at[s], dr.at[(fs % 2) * 8 + tp], (to(s), fs // 2)
        )

    @pl.loop(1, 1 + EARLY)
    def _(s):
        gate_copy(s).start()

    l_tok.wait()
    share = pl.ds(pl.multiple_of(tp * 256, 256), 256)

    @pl.loop(0, 12)
    def _(r):
        rows = pl.ds(pl.multiple_of(r * 64, 64), 64)
        v = tok[rows, :].astype(F32)
        inv = lax.rsqrt(jnp.mean(v * v, axis=-1, keepdims=True) + 1e-06)
        nrm[rows, :] = (tok[rows, share].astype(F32) * inv).astype(BF)

    s_id = lax.broadcasted_iota(jnp.int32, (CAP, 768), 0).astype(F32)

    def block(e):
        pick = jnp.where(s_id == pos_e[pl.ds(e, 1), :], 1.0, 0.0).astype(BF)
        return jnp.dot(pick, nrm[...], preferred_element_type=F32).astype(BF)

    def disp_copy(s):
        return rc(PS.at[s], X.at[fs, x, c], ps.at[s], xr.at[fs * 8 + tp], (to(s), tp))

    X[fs, x, c] = block(fs)

    @pl.loop(1, 17)
    def _(s):
        @pl.when(s < 16)
        def _():
            PS[s] = block(to(s))

        @pl.when(s > 1)
        def _():
            disp_copy(s - 1).start()

    @pl.loop(1 + EARLY, 16)
    def _(s):
        gate_copy(s).start()

    l_up.wait()

    @pl.loop(0, 16)
    def _(e):
        up_s[e] = (st_a[e] * gain).astype(BF)

    up_r[mine, :] = up_s[fs]

    @pl.loop(1, 16)
    def _(s):
        up_copy(s).start()

    l_down.wait()

    @pl.loop(0, 16)
    def _(e):
        down_s[e] = st_d[e].astype(BF)

    @pl.loop(1, 16)
    def _(s):
        down_copy(s).start()

    @pl.when(jnp.logical_not(self_down))
    def _():
        down_copy(0).start()

    @pl.when(self_down)
    def _():
        down_r[fs % 2, tp] = down_s[fs]

    def ag_copy(s, d, core, k, dev):
        i = of(s)
        p = at_x(d)
        return rc(X.at[i, p, core], X.at[i, p, core], ag.at[s * 7 + k], xr.at[i * 8 + p * 2 + core], dev)

    def ag_wait(s, d, core):
        ag_copy(s, d, core, 0, sib).wait_recv()

    def ahead(s):
        return 1 + 2 * (s % 2)

    @pl.loop(0, 20)
    def _(t):
        @pl.when(t < 16)
        def _():
            @pl.when(t > 0)
            def _():
                ag_wait(t, 0, c)

            ag_copy(t, 0, c, 0, (fs, lane(1, c))).start()
            ag_copy(t, 0, c, 1, (fs, lane(3, c))).start()
            ag_copy(t, 0, c, 2, sib).start()

        @pl.when(jnp.logical_and(t >= 2, t < 18))
        def _():
            s = t - 2
            da = ahead(s)
            ag_wait(s, 4 - da, c)
            ag_copy(s, 4 - da, c, 3, (fs, lane(da, c))).start()
            ag_copy(s, 4 - da, c, 4, sib).start()
            ag_wait(s, da, c)
            ag_copy(s, da, c, 5, sib).start()

        @pl.when(t >= 4)
        def _():
            s = t - 4
            ag_wait(s, 2, c)
            ag_copy(s, 2, c, 6, sib).start()

    @pl.loop(1, 16)
    def _(s):
        i = of(s)
        rows = pl.ds(pl.multiple_of(i * 128, 128), 128)
        rc(gate_s.at[0], gate_r.at[rows], gs.at[0], gr.at[i], sib).wait_recv()
        rc(up_s.at[0], up_r.at[rows], us.at[0], ur.at[i], sib).wait_recv()

    o_gate = pltpu.make_async_copy(gate_r, gate_o.at[0], osem.at[16])
    o_up = pltpu.make_async_copy(up_r, up_o.at[0], osem.at[17])
    o_gate.start()
    o_up.start()

    @pl.loop(0, 16)
    def _(s):
        i = of(s)
        for d in range(4):
            ag_wait(s, d, oc)
        rows = jnp.concatenate([X[i, p // 2, p % 2] for p in range(8)], axis=1)
        for h in range(2):
            g = jnp.dot(rows, gate_r[:, h * 256 : h * 256 + 256], preferred_element_type=F32)
            u = jnp.dot(rows, up_r[:, h * 256 : h * 256 + 256], preferred_element_type=F32)
            H[s, h] = (g / (1.0 + jnp.exp(-g)) * u).astype(BF)

    @pl.loop(0, 16)
    def _(k):
        h, j = k // 8, k % 8
        i = tp * 2 + h

        @pl.when(jnp.logical_or(i != fs, j != tp))
        def _():
            rc(down_s.at[0], down_r.at[h, j], ds.at[0], dr.at[k], sib).wait_recv()

    def o_down(k):
        h, j = k // 8, k % 8
        return pltpu.make_async_copy(
            down_r.at[h, j], down_o.at[0, pl.ds(h * 256, 256), pl.ds(j * 256, 256)], osem.at[k]
        )

    for k in range(16):
        o_down(k).start()

    acc[...] = jnp.zeros_like(acc)

    def pair_copy(s):
        return rc(X.at[of(s), :, oc], RB.at[s], dds.at[s], ddr.at[s], sib)

    def far_copy(s):
        return rc(X.at[of(s), at_x(2), c], D2.at[s], s2s.at[s], s2r.at[s], (fs, lane(ahead(s), c)))

    def a_copy(s):
        return rc(
            X.at[of(s), at_x(ahead(s)), c], FA.at[s], sas.at[s], sar.at[s], (fs, lane(ahead(s), c))
        )

    def b_copy(s):
        return rc(
            X.at[of(s), at_x(4 - ahead(s)), c], FB.at[s], sbs.at[s], sbr.at[s], (fs, lane(4 - ahead(s), c))
        )

    def ret_copy(s):
        return rc(X.at[of(s), x, c], RET.at[fs], rts.at[s], rtr.at[fs], (of(s), tp))

    LAGS = (0, 1, 3, 5, 8)

    def stage(t, k, low=0):
        s = t - LAGS[k]
        return jnp.logical_and(s >= low, s < 16), s

    @pl.loop(0, 16 + LAGS[4])
    def _(t):
        on3, s3 = stage(t, 3)
        on2, s2 = stage(t, 2)
        on1, s1 = stage(t, 1)
        on0, s0 = stage(t, 0)
        on4, s4 = stage(t, 4)

        @pl.when(on3)
        def _():
            a_copy(s3).wait_recv()
            b_copy(s3).wait_recv()
            i = of(s3)
            X[i, x, c] = (X[i, x, c].astype(F32) + FA[s3].astype(F32) + FB[s3].astype(F32)).astype(BF)

        @pl.when(on2)
        def _():
            far_copy(s2).wait_recv()
            i, p = of(s2), at_x(ahead(s2))
            X[i, p, c] = (X[i, p, c].astype(F32) + D2[s2].astype(F32)).astype(BF)

        @pl.when(on1)
        def _():
            pair_copy(s1).wait_recv()
            i = of(s1)
            for p in range(4):
                X[i, p, c] = (X[i, p, c].astype(F32) + RB[s1, p].astype(F32)).astype(BF)

        @pl.when(on0)
        def _():
            for k in range(7):
                ag_copy(s0, 0, c, k, sib).wait_send()
            i = of(s0)
            hid = jnp.concatenate([H[s0, 0], H[s0, 1]], axis=1)
            for j in range(8):
                w = jnp.concatenate([down_r[0, j], down_r[1, j]], axis=0)
                X[i, j // 2, j % 2] = jnp.dot(hid, w, preferred_element_type=F32).astype(BF)

        @pl.when(on3)
        def _():
            @pl.when(s3 > 0)
            def _():
                ret_copy(s3).start()

            @pl.when(s3 == 0)
            def _():
                RET[fs] = X[fs, x, c]

        @pl.when(on2)
        def _():
            a_copy(s2).start()

        @pl.when(on1)
        def _():
            far_copy(s1).start()
            b_copy(s1).start()

        @pl.when(on0)
        def _():
            pair_copy(s0).start()

        @pl.when(on4)
        def _():
            e = to(s4)

            @pl.when(s4 > 0)
            def _():
                rc(X.at[0, 0, 0], RET.at[e], rts.at[0], rtr.at[e], sib).wait_recv()

            want = lax.broadcasted_iota(jnp.int32, (768, CAP), 1) + e * CAP
            k0 = cols[:, 0:1].astype(jnp.int32)
            k1 = cols[:, 1:2].astype(jnp.int32)
            w = jnp.where(want == k0, cols[:, 2:3], jnp.where(want == k1, cols[:, 3:4], 0.0))
            hi = w.astype(BF)
            lo = (w - hi.astype(F32)).astype(BF)
            back = RET[e]
            acc[...] += jnp.dot(hi, back, preferred_element_type=F32) + jnp.dot(
                lo, back, preferred_element_type=F32
            )

    out_ref[...] = acc[...].astype(BF)

    o_gate.wait()
    o_up.wait()
    for k in range(16):
        o_down(k).wait()

    @pl.loop(1, 16)
    def _(s):
        gate_copy(s).wait_send()
        up_copy(s).wait_send()
        down_copy(s).wait_send()
        disp_copy(s).wait_send()
        ret_copy(s).wait_send()

    @pl.when(jnp.logical_not(self_down))
    def _():
        down_copy(0).wait_send()

    @pl.loop(0, 16)
    def _(s):
        pair_copy(s).wait_send()
        far_copy(s).wait_send()
        a_copy(s).wait_send()
        b_copy(s).wait_send()


def body(tokens, routes, route_weight, norm_gain, gate_master, up_master, down_master):
    hbm = pl.BlockSpec(memory_space=pl.ANY)
    vm = pl.BlockSpec(memory_space=pltpu.VMEM)
    dma = pltpu.SemaphoreType.DMA
    piece = (16, CAP, 256)
    return tuple(
        pl.pallas_call(
            kernel,
            name="experts",
            out_shape=(
                jax.ShapeDtypeStruct((1, 2048, 512), BF),
                jax.ShapeDtypeStruct((1, 2048, 512), BF),
                jax.ShapeDtypeStruct((1, 512, 2048), BF),
                jax.ShapeDtypeStruct((768, 256), BF),
            ),
            in_specs=[hbm, vm, vm, vm, hbm, hbm, hbm],
            out_specs=(hbm, hbm, hbm, vm),
            scratch_shapes=[
                pltpu.VMEM((16, 4, 2, CAP, 256), BF),
                pltpu.VMEM((16, 4, CAP, 256), BF),
                pltpu.VMEM(piece, BF),
                pltpu.VMEM(piece, BF),
                pltpu.VMEM(piece, BF),
                pltpu.VMEM(piece, BF),
                pltpu.VMEM(piece, BF),
                pltpu.VMEM((16, 2, CAP, 256), BF),
                pltpu.VMEM((16, 128, 512), BF),
                pltpu.VMEM((16, 128, 512), BF),
                pltpu.VMEM((16, 256, 256), BF),
                pltpu.VMEM((2048, 512), BF),
                pltpu.VMEM((2048, 512), BF),
                pltpu.VMEM((2, 8, 256, 256), BF),
                pltpu.VMEM((16, 128, 512), F32),
                pltpu.VMEM((16, 256, 256), F32),
                pltpu.VMEM((768, 2048), BF),
                pltpu.VMEM((768, 256), BF),
                pltpu.VMEM((768, 256), F32),
                pltpu.VMEM((16, 768), F32),
                pltpu.VMEM((768, 128), F32),
                dma((4,)),
                *[dma((16,))] * 7,
                dma((128,)),
                dma((112,)),
                *[dma((16,))] * 10,
                dma((18,)),
            ],
            compiler_params=pltpu.CompilerParams(
                collective_id=0, has_side_effects=True, vmem_limit_bytes=67043328
            ),
        )(
            tokens,
            routes.T,
            route_weight.T,
            norm_gain.reshape(1, 128),
            gate_master,
            up_master,
            down_master,
        )
    )


def solution(mesh):
    placed = (
        P("fs", None),
        P("fs", None),
        P("fs", None),
        P("fs"),
        P(None, "fs", "tp"),
        P(None, "fs", "tp"),
        P(None, "fs", "tp"),
    )
    return jax.shard_map(
        body,
        mesh=mesh,
        in_specs=placed,
        out_specs=(P("fs", None, "tp"), P("fs", None, "tp"), P("fs", "tp", None), P("fs", "tp")),
        check_vma=False,
    )
```

time: 409 us -> 295 us (0.72); the launches traced: 403 us -> 294 us
  Pallas kernels: 0 us -> 286 us
  waiting for transfers between devices: 125 us -> 0 us
  local copies, waits for them, and re-layouts: 92 us -> 7.61 us
  blocking collectives: 62.5 us -> 0 us
  other arithmetic: 48.4 us -> 0 us
  matrix products: 34.9 us -> 0 us
  starting transfers between devices: 26.6 us -> 0 us
  between operations: 14.2 us -> 0.65 us
    pallas_call x0 -> x1, Pallas kernels: none -> 286 us  [body(): pl.pallas_call(kernel, name='experts', out_shape=(jax.ShapeDtypeStruct((1...]
    reduce_scatter x1 -> x0, waiting for transfers between devices: 78.2 us -> none  [body(): lax.psum_scatter(rounded.astype(jnp.bfloat16), 'tp', scatter_dimension=2,...]
    all_to_all x2 -> x0, blocking collectives: 62.5 us -> none  [the longest x1 31.5 us: relay_down(): lax.all_to_all(lax.all_to_all(down_cast, 'fs', split_axis=0, concat_axis=...]
    all_to_all x4 -> x0, waiting for transfers between devices: 46.6 us -> none  [the longest x1 20.1 us: body(): lax.all_to_all(summed, 'fs', split_axis=0, concat_axis=0, tiled=True)]
    dot_general x2 -> x0, matrix products: 34.9 us -> none  [the longest x1 21.7 us: body(): jnp.dot(hidden, down_serve[0], preferred_element_type=jnp.float32)]
    all_to_all x2 -> x0, local copies, waits for them, and re-layouts: 27.5 us -> none  [the longest x1 25.1 us: relay_down(): lax.all_to_all(down_cast, 'fs', split_axis=0, concat_axis=1, tiled=True)]
    all_to_all x4 -> x0, starting transfers between devices: 26.3 us -> none  [the longest x1 7.35 us: body(): lax.all_to_all(summed, 'fs', split_axis=0, concat_axis=0, tiled=True)]
    unnamed x1 -> x0, other arithmetic: 21.6 us -> none
  transfers between devices with their start and end apart: 6 -> 0, of which waited for: 4 -> 0; matrix products, arithmetic and copies ran while one was open for 22% -> 0% of each run, Pallas kernels for 0% -> 0%
where the time goes in v1:
time: 295 us; the launch traced here: 294 us
  Pallas kernels  286 us (97%)
  local copies, waits for them, and re-layouts  7.61 us (3%)
    pallas_call x1, Pallas kernels, body(): pl.pallas_call(kernel, name='experts', out_shape=(jax.ShapeDtypeStruct((1...  286 us
    unnamed x10, local copies, waits for them, and re-layouts  7.61 us

profile of v1, /device:TPU:32, one launch (start us, length us, event | category | flops | bytes accessed | tf_op | source)
XLA Modules:
  0.0 293.8 jit_solution(10691349487427879787)
XLA Ops:
  0.6 285.5 %experts.1 = (bf16[1,2048,512]{2,1,0:T(8,128)(2,1)}, bf16[1,2048,512]{2,1,0:T(8,128)(2,1)}, bf16[1,512,2048]{2,1,0:T(8,128)(2,1)}, bf16[768,256]{1,0:T(8,128)(2,1)}) custom-call(bf16[768,2048]{1,0:T(8,128)(2,1)} %tok_h.1, s32[2,768]{1,0:T(2,128)} %bitcast.3, f32[2,768]{1,0:T(2,128)} %bitcast.4, f32[1,128]{1,0:T(1,128)} %bitcast.5, f32[16,128,512]{2,1,0:T(8,128)} %gate_h.1, ...), custom_call_target="tpu_custom_call" | custom-call | tf_op jit(solution)/shard_map/experts/pallas_call | solution.py:432
  286.2 0.0 copy-start.1
  286.2 3.2 %copy.15 = bf16[1,2048,512]{2,1,0:T(8,128)(2,1)} copy(bf16[1,2048,512]{2,1,0:T(8,128)(2,1)} %get-tuple-element.8) | data formatting | bytes 4194304
  289.4 0.0 copy-done.1
  289.4 0.0 copy-start
  289.4 1.3 copy.16
  290.7 1.0 copy-done
  291.7 0.0 copy-start.2
  291.7 1.3 copy.17
  293.1 0.0 copy-done.2
  293.1 0.7 copy.18
Async XLA Ops:
  286.2 3.2 %copy-start.1 = (bf16[1,2048,512]{2,1,0:T(8,128)(2,1)S(1)}, bf16[1,2048,512]{2,1,0:T(8,128)(2,1)}, u32[]{:S(2)}) copy-start(bf16[1,2048,512]{2,1,0:T(8,128)(2,1)} %get-tuple-element.9) | copy-start | bytes 6291460
  289.4 2.3 copy-start
  291.7 1.3 copy-start.2

commit v2 on v1

--- a/solution.py
+++ b/solution.py
@@ -19,8 +19,8 @@
     gate_o, up_o, down_o, out_ref,
     X, RB, D2, FA, FB, RET, PS, H,
     gate_s, up_s, down_s, gate_r, up_r, down_r,
-    st_a, st_d, tok, nrm, acc, pos_e, cols,
-    ld, gs, gr, us, ur, ds, dr, ps, xr, ag,
+    DN, st_a, st_d, tok, nrm, acc, pos_e, cols,
+    ld, gs, gr, us, ur, ds, dr, es, er, ps, xr, ag,
     dds, ddr, s2s, s2r, sas, sar, sbs, sbr, rts, rtr, osem,
 ):
     fs, tp = lax.axis_index("fs"), lax.axis_index("tp")
@@ -64,28 +64,13 @@
     def sig(dev):
         pl.semaphore_signal(bar, inc=1, device_id=dev, device_id_type=MESH)
 
-    self_down = fs // 2 == tp
-
     @pl.loop(1, 16)
     def _(s):
         sig((to(s), tp))
-        sig((to(s), fs // 2))
-
-    sig(sib)
-    sig((fs, lane(1, c)))
-    sig((fs, lane(3, c)))
-
-    @pl.when(jnp.logical_not(self_down))
-    def _():
-        sig((fs, fs // 2))
-
-    @pl.loop(0, 16)
+
+    @pl.loop(1, 8)
     def _(k):
-        i, j = tp * 2 + k // 8, k % 8
-
-        @pl.when(jnp.logical_or(i != fs, j != tp))
-        def _():
-            sig((i, j))
+        sig((fs, (tp + k) % 8))
 
     e_id = lax.broadcasted_iota(jnp.int32, (16, 768), 0)
     m0 = e_id == rt_ref[0:1, :]
@@ -121,13 +106,7 @@
     gate_r[mine, :] = gate_s[fs]
     l_up.start()
 
-    @pl.when(self_down)
-    def _():
-        pl.semaphore_wait(bar, 48)
-
-    @pl.when(jnp.logical_not(self_down))
-    def _():
-        pl.semaphore_wait(bar, 50)
+    pl.semaphore_wait(bar, 22)
 
     def gate_copy(s):
         return rc(gate_s.at[to(s)], gate_r.at[mine], gs.at[s], gr.at[fs], (to(s), tp))
@@ -136,9 +115,10 @@
         return rc(up_s.at[to(s)], up_r.at[mine], us.at[s], ur.at[fs], (to(s), tp))
 
     def down_copy(s):
-        return rc(
-            down_s.at[to(s)], down_r.at[fs % 2, tp], ds.at[s], dr.at[(fs % 2) * 8 + tp], (to(s), fs // 2)
-        )
+        return rc(down_s.at[to(s)], DN.at[fs], es.at[s], er.at[fs], (to(s), tp))
+
+    def down_on(i):
+        return rc(DN.at[i], down_r.at[i % 2, tp], ds.at[i], dr.at[(i % 2) * 8 + tp], (fs, i // 2))
 
     @pl.loop(1, 1 + EARLY)
     def _(s):
@@ -175,9 +155,17 @@
         def _():
             disp_copy(s - 1).start()
 
-    @pl.loop(1 + EARLY, 16)
-    def _(s):
-        gate_copy(s).start()
+    l_down.wait()
+
+    @pl.loop(0, 16)
+    def _(e):
+        down_s[e] = st_d[e].astype(BF)
+
+    @pl.loop(1, 16)
+    def _(s):
+        down_copy(s).start()
+
+    DN[fs] = down_s[fs]
 
     l_up.wait()
 
@@ -186,28 +174,6 @@
         up_s[e] = (st_a[e] * gain).astype(BF)
 
     up_r[mine, :] = up_s[fs]
-
-    @pl.loop(1, 16)
-    def _(s):
-        up_copy(s).start()
-
-    l_down.wait()
-
-    @pl.loop(0, 16)
-    def _(e):
-        down_s[e] = st_d[e].astype(BF)
-
-    @pl.loop(1, 16)
-    def _(s):
-        down_copy(s).start()
-
-    @pl.when(jnp.logical_not(self_down))
-    def _():
-        down_copy(0).start()
-
-    @pl.when(self_down)
-    def _():
-        down_r[fs % 2, tp] = down_s[fs]
 
     def ag_copy(s, d, core, k, dev):
         i = of(s)
@@ -231,6 +197,14 @@
             ag_copy(t, 0, c, 0, (fs, lane(1, c))).start()
             ag_copy(t, 0, c, 1, (fs, lane(3, c))).start()
             ag_copy(t, 0, c, 2, sib).start()
+
+        @pl.when(jnp.logical_and(t >= 4, t < 19 - EARLY))
+        def _():
+            gate_copy(t - 3 + EARLY).start()
+
+        @pl.when(t >= 5)
+        def _():
+            up_copy(t - 4).start()
 
         @pl.when(jnp.logical_and(t >= 2, t < 18))
         def _():
@@ -248,6 +222,22 @@
             ag_wait(s, 2, c)
             ag_copy(s, 2, c, 6, sib).start()
 
+    @pl.loop(0, 16)
+    def _(s):
+        i = of(s)
+
+        @pl.when(s > 0)
+        def _():
+            rc(down_s.at[0], DN.at[i], es.at[0], er.at[i], sib).wait_recv()
+
+        @pl.when(i // 2 != tp)
+        def _():
+            down_on(i).start()
+
+        @pl.when(i // 2 == tp)
+        def _():
+            down_r[i % 2, tp] = DN[i]
+
     @pl.loop(1, 16)
     def _(s):
         i = of(s)
@@ -261,24 +251,10 @@
     o_up.start()
 
     @pl.loop(0, 16)
-    def _(s):
-        i = of(s)
-        for d in range(4):
-            ag_wait(s, d, oc)
-        rows = jnp.concatenate([X[i, p // 2, p % 2] for p in range(8)], axis=1)
-        for h in range(2):
-            g = jnp.dot(rows, gate_r[:, h * 256 : h * 256 + 256], preferred_element_type=F32)
-            u = jnp.dot(rows, up_r[:, h * 256 : h * 256 + 256], preferred_element_type=F32)
-            H[s, h] = (g / (1.0 + jnp.exp(-g)) * u).astype(BF)
-
-    @pl.loop(0, 16)
     def _(k):
-        h, j = k // 8, k % 8
-        i = tp * 2 + h
-
-        @pl.when(jnp.logical_or(i != fs, j != tp))
-        def _():
-            rc(down_s.at[0], down_r.at[h, j], ds.at[0], dr.at[k], sib).wait_recv()
+        @pl.when(k % 8 != tp)
+        def _():
+            rc(DN.at[0], down_r.at[k // 8, k % 8], ds.at[0], dr.at[k], sib).wait_recv()
 
     def o_down(k):
         h, j = k // 8, k % 8
@@ -310,7 +286,7 @@
     def ret_copy(s):
         return rc(X.at[of(s), x, c], RET.at[fs], rts.at[s], rtr.at[fs], (of(s), tp))
 
-    LAGS = (0, 1, 3, 5, 8)
+    LAGS = (0, 2, 5, 8, 11)
 
     def stage(t, k, low=0):
         s = t - LAGS[k]
@@ -318,11 +294,34 @@
 
     @pl.loop(0, 16 + LAGS[4])
     def _(t):
+        on4, s4 = stage(t, 4)
         on3, s3 = stage(t, 3)
         on2, s2 = stage(t, 2)
         on1, s1 = stage(t, 1)
         on0, s0 = stage(t, 0)
-        on4, s4 = stage(t, 4)
+
+        @pl.when(on2)
+        def _():
+            far_copy(s2).wait_recv()
+            i, p = of(s2), at_x(ahead(s2))
+            X[i, p, c] = (X[i, p, c].astype(F32) + D2[s2].astype(F32)).astype(BF)
+
+        @pl.when(on1)
+        def _():
+            pair_copy(s1).wait_recv()
+            i = of(s1)
+            for d in (2, 4 - ahead(s1), ahead(s1), 0):
+                p = at_x(d)
+                X[i, p, c] = (X[i, p, c].astype(F32) + RB[s1, p].astype(F32)).astype(BF)
+
+        @pl.when(on2)
+        def _():
+            a_copy(s2).start()
+
+        @pl.when(on1)
+        def _():
+            far_copy(s1).start()
+            b_copy(s1).start()
 
         @pl.when(on3)
         def _():
@@ -331,25 +330,19 @@
             i = of(s3)
             X[i, x, c] = (X[i, x, c].astype(F32) + FA[s3].astype(F32) + FB[s3].astype(F32)).astype(BF)
 
-        @pl.when(on2)
-        def _():
-            far_copy(s2).wait_recv()
-            i, p = of(s2), at_x(ahead(s2))
-            X[i, p, c] = (X[i, p, c].astype(F32) + D2[s2].astype(F32)).astype(BF)
-
-        @pl.when(on1)
-        def _():
-            pair_copy(s1).wait_recv()
-            i = of(s1)
-            for p in range(4):
-                X[i, p, c] = (X[i, p, c].astype(F32) + RB[s1, p].astype(F32)).astype(BF)
-
         @pl.when(on0)
         def _():
             for k in range(7):
                 ag_copy(s0, 0, c, k, sib).wait_send()
             i = of(s0)
-            hid = jnp.concatenate([H[s0, 0], H[s0, 1]], axis=1)
+            for d in range(4):
+                ag_wait(s0, d, oc)
+            rows = jnp.concatenate([X[i, p // 2, p % 2] for p in range(8)], axis=1)
+            for h in range(2):
+                g = jnp.dot(rows, gate_r[:, h * 256 : h * 256 + 256], preferred_element_type=F32)
+                u = jnp.dot(rows, up_r[:, h * 256 : h * 256 + 256], preferred_element_type=F32)
+                H[h] = (g / (1.0 + jnp.exp(-g)) * u).astype(BF)
+            hid = jnp.concatenate([H[0], H[1]], axis=1)
             for j in range(8):
                 w = jnp.concatenate([down_r[0, j], down_r[1, j]], axis=0)
                 X[i, j // 2, j % 2] = jnp.dot(hid, w, preferred_element_type=F32).astype(BF)
@@ -363,15 +356,6 @@
             @pl.when(s3 == 0)
             def _():
                 RET[fs] = X[fs, x, c]
-
-        @pl.when(on2)
-        def _():
-            a_copy(s2).start()
-
-        @pl.when(on1)
-        def _():
-            far_copy(s1).start()
-            b_copy(s1).start()
 
         @pl.when(on0)
         def _():
@@ -411,9 +395,11 @@
         disp_copy(s).wait_send()
         ret_copy(s).wait_send()
 
-    @pl.when(jnp.logical_not(self_down))
-    def _():
-        down_copy(0).wait_send()
+    @pl.loop(0, 16)
+    def _(i):
+        @pl.when(i // 2 != tp)
+        def _():
+            down_on(i).wait_send()
 
     @pl.loop(0, 16)
     def _(s):
@@ -421,6 +407,32 @@
         far_copy(s).wait_send()
         a_copy(s).wait_send()
         b_copy(s).wait_send()
+
+
+def settle(*refs):
+    src, dst, bufs, (rd, wr) = refs[:4], refs[4:8], refs[8:12], refs[12:]
+    parts = [(k, h) for h in range(2) for k in range(4)]
+
+    def half(k, h, ref):
+        ref = ref.at[0] if k < 3 else ref
+        n = (1024, 1024, 256, 384)[k]
+        return ref.at[h * n : h * n + n]
+
+    def get(n):
+        k, h = parts[n]
+        return pltpu.make_async_copy(half(k, h, src[k]), half(k, h, bufs[k]), rd.at[n])
+
+    def put(n):
+        k, h = parts[n]
+        return pltpu.make_async_copy(half(k, h, bufs[k]), half(k, h, dst[k]), wr.at[n])
+
+    for n in range(8):
+        get(n).start()
+    for n in range(8):
+        get(n).wait()
+        put(n).start()
+    for n in range(8):
+        put(n).wait()
 
 
 def body(tokens, routes, route_weight, norm_gain, gate_master, up_master, down_master):
@@ -428,7 +440,7 @@
     vm = pl.BlockSpec(memory_space=pltpu.VMEM)
     dma = pltpu.SemaphoreType.DMA
     piece = (16, CAP, 256)
-    return tuple(
+    held = tuple(
         pl.pallas_call(
             kernel,
             name="experts",
@@ -448,13 +460,14 @@
                 pltpu.VMEM(piece, BF),
                 pltpu.VMEM(piece, BF),
                 pltpu.VMEM(piece, BF),
-                pltpu.VMEM((16, 2, CAP, 256), BF),
+                pltpu.VMEM((2, CAP, 256), BF),
                 pltpu.VMEM((16, 128, 512), BF),
                 pltpu.VMEM((16, 128, 512), BF),
                 pltpu.VMEM((16, 256, 256), BF),
                 pltpu.VMEM((2048, 512), BF),
                 pltpu.VMEM((2048, 512), BF),
                 pltpu.VMEM((2, 8, 256, 256), BF),
+                pltpu.VMEM((16, 256, 256), BF),
                 pltpu.VMEM((16, 128, 512), F32),
                 pltpu.VMEM((16, 256, 256), F32),
                 pltpu.VMEM((768, 2048), BF),
@@ -463,7 +476,7 @@
                 pltpu.VMEM((16, 768), F32),
                 pltpu.VMEM((768, 128), F32),
                 dma((4,)),
-                *[dma((16,))] * 7,
+                *[dma((16,))] * 9,
                 dma((128,)),
                 dma((112,)),
                 *[dma((16,))] * 10,
@@ -482,6 +495,17 @@
             down_master,
         )
     )
+    shapes = tuple(jax.ShapeDtypeStruct(v.shape, v.dtype) for v in held)
+    return tuple(
+        pl.pallas_call(
+            settle,
+            name="settle",
+            out_shape=shapes,
+            in_specs=[hbm] * 4,
+            out_specs=(hbm,) * 4,
+            scratch_shapes=[*[pltpu.VMEM(v.shape, v.dtype) for v in held], dma((8,)), dma((8,))],
+        )(*held)
+    )
 
 
 def solution(mesh):

time: 295 us -> 193 us (0.65)
  Pallas kernels: 286 us -> 192 us
  local copies, waits for them, and re-layouts: 7.61 us -> 0 us
    pallas_call x1, Pallas kernels: 286 us -> 186 us  [body(): pl.pallas_call(kernel, name='experts', out_shape=(jax.ShapeDtypeStruct((1...]
    unnamed x10 -> x0, local copies, waits for them, and re-layouts: 7.61 us -> none
    pallas_call x0 -> x1, Pallas kernels: none -> 5.61 us  [body(): pl.pallas_call(settle, name='settle', out_shape=shapes, in_specs=[hbm] *...]
where the time goes in v2:
time: 193 us
  Pallas kernels  192 us (99%)
    pallas_call x1, Pallas kernels, body(): pl.pallas_call(kernel, name='experts', out_shape=(jax.ShapeDtypeStruct((1...  186 us
    pallas_call x1, Pallas kernels, body(): pl.pallas_call(settle, name='settle', out_shape=shapes, in_specs=[hbm] *...  5.61 us

profile of v2, /device:TPU:32, one launch (start us, length us, event | category | flops | bytes accessed | tf_op | source)
XLA Modules:
  0.0 192.6 jit_solution(6850322549618534692)
XLA Ops:
  0.6 186.4 %experts.1 = (bf16[1,2048,512]{2,1,0:T(8,128)(2,1)}, bf16[1,2048,512]{2,1,0:T(8,128)(2,1)}, bf16[1,512,2048]{2,1,0:T(8,128)(2,1)}, bf16[768,256]{1,0:T(8,128)(2,1)}) custom-call(bf16[768,2048]{1,0:T(8,128)(2,1)} %tok_h.1, s32[2,768]{1,0:T(2,128)} %bitcast.3, f32[2,768]{1,0:T(2,128)} %bitcast.4, f32[1,128]{1,0:T(1,128)} %bitcast.5, f32[16,128,512]{2,1,0:T(8,128)} %gate_h.1, ...), custom_call_target="tpu_custom_call" | custom-call | tf_op jit(solution)/shard_map/experts/pallas_call | solution.py:444
  187.0 5.6 %settle.1 = (bf16[1,2048,512]{2,1,0:T(8,128)(2,1)}, bf16[1,2048,512]{2,1,0:T(8,128)(2,1)}, bf16[1,512,2048]{2,1,0:T(8,128)(2,1)}, bf16[768,256]{1,0:T(8,128)(2,1)}) custom-call(bf16[1,2048,512]{2,1,0:T(8,128)(2,1)} %get-tuple-element.8.refs_0_, bf16[1,2048,512]{2,1,0:T(8,128)(2,1)} %get-tuple-element.9.refs_1_, ...), custom_call_target="tpu_custom_call" | custom-call | tf_op jit(solution)/shard_map/settle/pallas_call | solution.py:500

commit v3 on v2

--- a/solution.py
+++ b/solution.py
@@ -16,12 +16,12 @@
 
 def kernel(
     tok_h, rt_ref, wt_ref, gain_ref, gate_h, up_h, down_h,
-    gate_o, up_o, down_o, out_ref,
+    gate_r, up_r, down_r, out_ref,
     X, RB, D2, FA, FB, RET, PS, H,
-    gate_s, up_s, down_s, gate_r, up_r, down_r,
+    gate_s, up_s, down_s,
     DN, st_a, st_d, tok, nrm, acc, pos_e, cols,
     ld, gs, gr, us, ur, ds, dr, es, er, ps, xr, ag,
-    dds, ddr, s2s, s2r, sas, sar, sbs, sbr, rts, rtr, osem,
+    dds, ddr, s2s, s2r, sas, sar, sbs, sbr, rts, rtr,
 ):
     fs, tp = lax.axis_index("fs"), lax.axis_index("tp")
     z, y = fs // 4, fs % 4
@@ -117,8 +117,13 @@
     def down_copy(s):
         return rc(down_s.at[to(s)], DN.at[fs], es.at[s], er.at[fs], (to(s), tp))
 
+    def down_at(h, j):
+        return down_r.at[
+            pl.ds(pl.multiple_of(h * 256, 256), 256), pl.ds(pl.multiple_of(j * 256, 256), 256)
+        ]
+
     def down_on(i):
-        return rc(DN.at[i], down_r.at[i % 2, tp], ds.at[i], dr.at[(i % 2) * 8 + tp], (fs, i // 2))
+        return rc(DN.at[i], down_at(i % 2, tp), ds.at[i], dr.at[(i % 2) * 8 + tp], (fs, i // 2))
 
     @pl.loop(1, 1 + EARLY)
     def _(s):
@@ -184,7 +189,7 @@
         ag_copy(s, d, core, 0, sib).wait_recv()
 
     def ahead(s):
-        return 1 + 2 * (s % 2)
+        return 1 + 2 * ((s + c) % 2)
 
     @pl.loop(0, 20)
     def _(t):
@@ -236,7 +241,7 @@
 
         @pl.when(i // 2 == tp)
         def _():
-            down_r[i % 2, tp] = DN[i]
+            down_at(i % 2, tp)[...] = DN[i]
 
     @pl.loop(1, 16)
     def _(s):
@@ -245,25 +250,11 @@
         rc(gate_s.at[0], gate_r.at[rows], gs.at[0], gr.at[i], sib).wait_recv()
         rc(up_s.at[0], up_r.at[rows], us.at[0], ur.at[i], sib).wait_recv()
 
-    o_gate = pltpu.make_async_copy(gate_r, gate_o.at[0], osem.at[16])
-    o_up = pltpu.make_async_copy(up_r, up_o.at[0], osem.at[17])
-    o_gate.start()
-    o_up.start()
-
     @pl.loop(0, 16)
     def _(k):
         @pl.when(k % 8 != tp)
         def _():
-            rc(DN.at[0], down_r.at[k // 8, k % 8], ds.at[0], dr.at[k], sib).wait_recv()
-
-    def o_down(k):
-        h, j = k // 8, k % 8
-        return pltpu.make_async_copy(
-            down_r.at[h, j], down_o.at[0, pl.ds(h * 256, 256), pl.ds(j * 256, 256)], osem.at[k]
-        )
-
-    for k in range(16):
-        o_down(k).start()
+            rc(DN.at[0], down_at(k // 8, k % 8), ds.at[0], dr.at[k], sib).wait_recv()
 
     acc[...] = jnp.zeros_like(acc)
 
@@ -344,7 +335,7 @@
                 H[h] = (g / (1.0 + jnp.exp(-g)) * u).astype(BF)
             hid = jnp.concatenate([H[0], H[1]], axis=1)
             for j in range(8):
-                w = jnp.concatenate([down_r[0, j], down_r[1, j]], axis=0)
+                w = down_r[:, j * 256 : j * 256 + 256]
                 X[i, j // 2, j % 2] = jnp.dot(hid, w, preferred_element_type=F32).astype(BF)
 
         @pl.when(on3)
@@ -382,11 +373,6 @@
 
     out_ref[...] = acc[...].astype(BF)
 
-    o_gate.wait()
-    o_up.wait()
-    for k in range(16):
-        o_down(k).wait()
-
     @pl.loop(1, 16)
     def _(s):
         gate_copy(s).wait_send()
@@ -409,30 +395,17 @@
         b_copy(s).wait_send()
 
 
-def settle(*refs):
-    src, dst, bufs, (rd, wr) = refs[:4], refs[4:8], refs[8:12], refs[12:]
-    parts = [(k, h) for h in range(2) for k in range(4)]
-
-    def half(k, h, ref):
-        ref = ref.at[0] if k < 3 else ref
-        n = (1024, 1024, 256, 384)[k]
-        return ref.at[h * n : h * n + n]
-
-    def get(n):
-        k, h = parts[n]
-        return pltpu.make_async_copy(half(k, h, src[k]), half(k, h, bufs[k]), rd.at[n])
-
-    def put(n):
-        k, h = parts[n]
-        return pltpu.make_async_copy(half(k, h, bufs[k]), half(k, h, dst[k]), wr.at[n])
-
-    for n in range(8):
-        get(n).start()
-    for n in range(8):
-        get(n).wait()
-        put(n).start()
-    for n in range(8):
-        put(n).wait()
+def settle(gate_v, up_v, down_v, out_v, gate_o, up_o, down_o, out_o, sem):
+    copies = [
+        pltpu.make_async_copy(gate_v, gate_o.at[0], sem.at[0]),
+        pltpu.make_async_copy(up_v, up_o.at[0], sem.at[1]),
+        pltpu.make_async_copy(down_v, down_o.at[0], sem.at[2]),
+        pltpu.make_async_copy(out_v, out_o, sem.at[3]),
+    ]
+    for copy in copies:
+        copy.start()
+    for copy in copies:
+        copy.wait()
 
 
 def body(tokens, routes, route_weight, norm_gain, gate_master, up_master, down_master):
@@ -440,18 +413,18 @@
     vm = pl.BlockSpec(memory_space=pltpu.VMEM)
     dma = pltpu.SemaphoreType.DMA
     piece = (16, CAP, 256)
-    held = tuple(
+    gate_serve, up_serve, down_serve, layer_out = (
         pl.pallas_call(
             kernel,
             name="experts",
             out_shape=(
-                jax.ShapeDtypeStruct((1, 2048, 512), BF),
-                jax.ShapeDtypeStruct((1, 2048, 512), BF),
-                jax.ShapeDtypeStruct((1, 512, 2048), BF),
-                jax.ShapeDtypeStruct((768, 256), BF),
+                pltpu.VMEM((2048, 512), BF),
+                pltpu.VMEM((2048, 512), BF),
+                pltpu.VMEM((512, 2048), BF),
+                pltpu.VMEM((768, 256), BF),
             ),
             in_specs=[hbm, vm, vm, vm, hbm, hbm, hbm],
-            out_specs=(hbm, hbm, hbm, vm),
+            out_specs=(vm, vm, vm, vm),
             scratch_shapes=[
                 pltpu.VMEM((16, 4, 2, CAP, 256), BF),
                 pltpu.VMEM((16, 4, CAP, 256), BF),
@@ -464,9 +437,6 @@
                 pltpu.VMEM((16, 128, 512), BF),
                 pltpu.VMEM((16, 128, 512), BF),
                 pltpu.VMEM((16, 256, 256), BF),
-                pltpu.VMEM((2048, 512), BF),
-                pltpu.VMEM((2048, 512), BF),
-                pltpu.VMEM((2, 8, 256, 256), BF),
                 pltpu.VMEM((16, 256, 256), BF),
                 pltpu.VMEM((16, 128, 512), F32),
                 pltpu.VMEM((16, 256, 256), F32),
@@ -480,10 +450,9 @@
                 dma((128,)),
                 dma((112,)),
                 *[dma((16,))] * 10,
-                dma((18,)),
             ],
             compiler_params=pltpu.CompilerParams(
-                collective_id=0, has_side_effects=True, vmem_limit_bytes=67043328
+                collective_id=0, has_side_effects=True, vmem_limit_bytes=60000000
             ),
         )(
             tokens,
@@ -495,15 +464,24 @@
             down_master,
         )
     )
-    shapes = tuple(jax.ShapeDtypeStruct(v.shape, v.dtype) for v in held)
+    held = [
+        pltpu.with_memory_space_constraint(v, pltpu.VMEM)
+        for v in (gate_serve, up_serve, down_serve, layer_out)
+    ]
     return tuple(
         pl.pallas_call(
             settle,
             name="settle",
-            out_shape=shapes,
-            in_specs=[hbm] * 4,
+            out_shape=(
+                jax.ShapeDtypeStruct((1, 2048, 512), BF),
+                jax.ShapeDtypeStruct((1, 2048, 512), BF),
+                jax.ShapeDtypeStruct((1, 512, 2048), BF),
+                jax.ShapeDtypeStruct((768, 256), BF),
+            ),
+            in_specs=[vm] * 4,
             out_specs=(hbm,) * 4,
-            scratch_shapes=[*[pltpu.VMEM(v.shape, v.dtype) for v in held], dma((8,)), dma((8,))],
+            scratch_shapes=[dma((4,))],
+            compiler_params=pltpu.CompilerParams(vmem_limit_bytes=1 << 20),
         )(*held)
     )
 

time: 193 us -> 188 us (0.974)
  Pallas kernels: 192 us -> 187 us
    pallas_call x2, Pallas kernels: 192 us -> 187 us  [the longest x1 185 us: body(): pl.pallas_call(kernel, name='experts', out_shape=(pltpu.VMEM((2048, 512),...]
where the time goes in v3:
time: 188 us
  Pallas kernels  187 us (99%)
    pallas_call x1, Pallas kernels, body(): pl.pallas_call(kernel, name='experts', out_shape=(pltpu.VMEM((2048, 512),...  185 us

profile of v3, /device:TPU:32, one launch (start us, length us, event | category | flops | bytes accessed | tf_op | source)
XLA Modules:
  0.0 188.0 jit_solution(6763712319678970333)
XLA Ops:
  0.6 184.5 %experts.1 = (bf16[2048,512]{1,0:T(8,128)(2,1)S(1)}, bf16[2048,512]{1,0:T(8,128)(2,1)S(1)}, bf16[512,2048]{1,0:T(8,128)(2,1)S(1)}, bf16[768,256]{1,0:T(8,128)(2,1)S(1)}) custom-call(bf16[768,2048]{1,0:T(8,128)(2,1)} %tok_h.1, s32[2,768]{1,0:T(2,128)} %bitcast.3, f32[2,768]{1,0:T(2,128)} %bitcast.4, f32[1,128]{1,0:T(1,128)} %bitcast.5, ...), custom_call_target="tpu_custom_call" | custom-call | tf_op jit(solution)/shard_map/experts/pallas_call | solution.py:417
  185.2 2.8 %settle.1 = (bf16[1,2048,512]{2,1,0:T(8,128)(2,1)}, bf16[1,2048,512]{2,1,0:T(8,128)(2,1)}, bf16[1,512,2048]{2,1,0:T(8,128)(2,1)}, bf16[768,256]{1,0:T(8,128)(2,1)}) custom-call(bf16[2048,512]{1,0:T(8,128)(2,1)S(1)} %get-tuple-element.8.gate_v, bf16[2048,512]{1,0:T(8,128)(2,1)S(1)} %get-tuple-element.9.up_v, bf16[512,2048]{1,0:T(8,128)(2,1)S(1)} %get-tuple-element.10.down_v, ...), custom_call_target="tpu_custom_call" | custom-call | tf_op jit(solution)/shard_map/settle/pallas_call | solution.py:472
